TPU v7x, 32 devices: a whole 2x2x4 slice. The times are simulated.
32 devices in a mesh: ep: 8 (over z, y), tp: 4 (over x, core).
Axes of the slice: x: 2, y: 2, z: 4, core: 2. Of those that a mesh axis runs over, the one named last changes fastest.
Arguments:
- hidden: bfloat16 [512, 2048], P('ep'), may hold values from -10 to 10
- mix_gain: bfloat16 [2048], replicated, may hold values from 0.099609375 to 1.8984375
- proj_x: bfloat16 [2048, 2048], P('ep', 'tp'), may hold values from -0.125 to 0.125
- proj_y: bfloat16 [2048, 2048], P('ep', 'tp'), may hold values from -0.125 to 0.125
- conv_taps: bfloat16 [4, 2048], P(None, 'tp'), may hold values from -3 to 3
- input_gate: bfloat16 [32, 64, 64], P('tp'), may hold values from -0.75 to 0.75
- decay_gate: bfloat16 [32, 64, 64], P('tp'), may hold values from -0.75 to 0.75
- decay_param: float32 [2048], P('tp'), may hold values from 1 to 6
- proj_out: bfloat16 [2048, 2048], P('tp'), may hold values from -0.125 to 0.125
- conv_state: bfloat16 [512, 3, 2048], P('ep', None, 'tp'), may hold values from -6 to 6
- lru_state: float32 [512, 2048], P('ep', 'tp'), may hold values from -6 to 6
- ffn_gain: bfloat16 [2048], replicated, may hold values from 0.099609375 to 1.8984375
- routes: int32 [512, 2], P('ep'), may hold values from 0 to 7, all different within a row; in each aligned block of 64 rows (0 to 63, 64 to 127, ...) at most 18 rows name the same one
- route_weights: float32 [512, 2], P('ep'), may hold values from 0.2 to 1
- expert_gate: bfloat16 [8, 2048, 3072], P('ep', None, 'tp'), may hold values from -0.125 to 0.125
- expert_up: bfloat16 [8, 2048, 3072], P('ep', None, 'tp'), may hold values from -0.125 to 0.125
- expert_down: bfloat16 [8, 3072, 2048], P('ep', 'tp'), may hold values from -0.109375 to 0.109375
- dense_gate: bfloat16 [2048, 6144], P('tp', 'ep'), may hold values from -0.125 to 0.125
- dense_up: bfloat16 [2048, 6144], P('tp', 'ep'), may hold values from -0.125 to 0.125
- dense_down: bfloat16 [6144, 2048], P('ep', 'tp'), may hold values from -0.078125 to 0.078125
- branch_gate: float32 [2048], P('tp'), may hold values from -4 to 4
Outputs:
- new_hidden: bfloat16 [512, 2048], P('ep', 'tp')
- new_lru: float32 [512, 2048], P('ep', 'tp')
- new_conv: bfloat16 [512, 3, 2048], P('ep', None, 'tp')
Inputs may be any that keep to these rules, and one draw needn't show every extreme that they name: `routes`: each row names 2 different experts. In the 64 rows of one index of ep, no expert is named by more than 18 rows, a bound that some block reaches.
All inputs are finite; a program needn't handle non-finite values.
Results may differ from a plain program's by a relative error of at most 0.017.
Values may be sent and summed in bfloat16 or wider, within the bound.
A program may use at most 128 MiB of HBM per device.

v0:
```python
import jax
import jax.numpy as jnp
from jax import lax
from jax.sharding import PartitionSpec as P

epsilon = 1e-06
decay_scale = 8.0


def rms_scale(values, gain_vec):
    floats = values.astype(jnp.float32)
    meansq = jnp.mean(floats * floats, axis=-1, keepdims=True)
    return floats * lax.rsqrt(meansq + epsilon) * gain_vec.astype(jnp.float32)


def on_device(
    hidden,
    mix_gain,
    proj_x,
    proj_y,
    conv_taps,
    input_gate,
    decay_gate,
    decay_param,
    proj_out,
    conv_state,
    lru_state,
    ffn_gain,
    routes,
    route_weights,
    expert_gate,
    expert_up,
    expert_down,
    dense_gate,
    dense_up,
    dense_down,
    branch_gate,
):
    tok_rows = hidden.shape[0]
    ep_size = lax.axis_size("ep")
    tp_size = lax.axis_size("tp")
    col_width = hidden.shape[1] // tp_size
    col_start = lax.axis_index("tp") * col_width
    lru_local = lru_state.shape[1]
    normed = rms_scale(hidden, mix_gain).astype(jnp.bfloat16)
    spread = lax.all_to_all(normed, "ep", split_axis=1, concat_axis=0, tiled=True)
    weights_xy = jnp.concatenate([proj_x, proj_y], axis=1)
    projected = lax.psum_scatter(
        jnp.dot(spread, weights_xy, preferred_element_type=jnp.float32).astype(jnp.bfloat16),
        "ep",
        scatter_dimension=0,
        tiled=True,
    ).astype(jnp.float32)
    x_proj = projected[:, :lru_local].astype(jnp.bfloat16)
    y_proj = projected[:, lru_local:].astype(jnp.bfloat16)
    window = jnp.concatenate([conv_state, x_proj[:, None, :]], axis=1)
    conv_out = jnp.sum(
        window.astype(jnp.float32) * conv_taps.astype(jnp.float32)[None], axis=1
    ).astype(jnp.bfloat16)
    heads_here = input_gate.shape[0]
    block_size = input_gate.shape[1]
    heads_in = conv_out.reshape(tok_rows, heads_here, block_size)
    gate_in = jax.nn.sigmoid(
        jnp.einsum(
            "bhi,hij->bhj", heads_in, input_gate, preferred_element_type=jnp.float32
        ).reshape(tok_rows, lru_local)
    )
    gate_dec = jax.nn.sigmoid(
        jnp.einsum(
            "bhi,hij->bhj", heads_in, decay_gate, preferred_element_type=jnp.float32
        ).reshape(tok_rows, lru_local)
    )
    log_decay = decay_scale * gate_dec * jax.nn.log_sigmoid(decay_param)
    decay_rate = jnp.exp(log_decay)
    inject = jnp.sqrt(-jnp.expm1(2.0 * log_decay))
    new_lru = decay_rate * lru_state + inject * gate_in * conv_out.astype(jnp.float32)
    gated_out = (new_lru * jax.nn.gelu(y_proj.astype(jnp.float32))).astype(jnp.bfloat16)
    partial_value = jnp.dot(gated_out, proj_out, preferred_element_type=jnp.float32)
    mixer_sum = lax.psum_scatter(
        partial_value.astype(jnp.bfloat16), "tp", scatter_dimension=1, tiled=True
    ).astype(jnp.float32)
    own_hidden = lax.dynamic_slice_in_dim(hidden, col_start, col_width, 1)
    summed = (own_hidden.astype(jnp.float32) + mixer_sum).astype(jnp.bfloat16)
    whole_rows = lax.all_gather(summed, "tp", axis=1, tiled=True)
    ffn_in = rms_scale(whole_rows, ffn_gain).astype(jnp.bfloat16)
    ffn_cols = lax.dynamic_slice_in_dim(ffn_in, col_start, col_width, 1)
    top_count = routes.shape[1]
    local_experts = expert_gate.shape[0]
    experts_all = local_experts * ep_size
    capacity = tok_rows * top_count // experts_all + 2
    pair_expert = routes.reshape(-1)
    onehot = (pair_expert[:, None] == jnp.arange(experts_all, dtype=jnp.int32)[None, :]).astype(
        jnp.int32
    )
    slot_rank = jnp.sum((jnp.cumsum(onehot, axis=0) - onehot) * onehot, axis=1)
    slot_index = pair_expert * capacity + slot_rank
    select = (
        slot_index[:, None] == jnp.arange(experts_all * capacity, dtype=jnp.int32)[None, :]
    ).astype(jnp.bfloat16)
    pair_rows = jnp.repeat(ffn_in, top_count, axis=0)
    dispatch = jnp.einsum(
        "pe,pd->ed", select, pair_rows, preferred_element_type=jnp.float32
    ).astype(jnp.bfloat16)
    dispatch = dispatch.reshape(experts_all, capacity, ffn_in.shape[1])
    arrived = lax.all_to_all(dispatch, "ep", split_axis=0, concat_axis=0, tiled=True)
    items = arrived.shape[1]
    grouped = arrived.reshape(ep_size, local_experts, items, arrived.shape[2])
    gate_val = jnp.einsum(
        "sgid,gdf->sgif", grouped, expert_gate, preferred_element_type=jnp.float32
    )
    up_val = jnp.einsum("sgid,gdf->sgif", grouped, expert_up, preferred_element_type=jnp.float32)
    inner_act = (jax.nn.silu(gate_val) * up_val).astype(jnp.bfloat16)
    partial_out = jnp.einsum(
        "sgif,gfd->sgid", inner_act, expert_down, preferred_element_type=jnp.float32
    )
    reduced = lax.psum_scatter(
        partial_out.astype(jnp.bfloat16), "tp", scatter_dimension=3, tiled=True
    )
    flat_back = reduced.reshape(ep_size * local_experts, items, reduced.shape[3])
    returned = lax.all_to_all(flat_back, "ep", split_axis=0, concat_axis=0, tiled=True)
    weighted = select.astype(jnp.float32) * route_weights.reshape(-1)[:, None]
    per_token = jnp.sum(weighted.reshape(tok_rows, top_count, experts_all * capacity), axis=1)
    expert_sum = jnp.dot(
        per_token,
        returned.reshape(experts_all * capacity, col_width).astype(jnp.float32),
        precision=lax.Precision.HIGHEST,
    )
    dense_both = jnp.concatenate([dense_gate, dense_up], axis=1)
    ff_local = dense_gate.shape[1]
    dense_part = jnp.dot(
        lax.all_gather(ffn_cols, "ep", axis=0, tiled=True),
        dense_both,
        preferred_element_type=jnp.float32,
    )
    dense_full = lax.psum(dense_part.astype(jnp.bfloat16), "tp").astype(jnp.float32)
    dense_act = (jax.nn.silu(dense_full[:, :ff_local]) * dense_full[:, ff_local:]).astype(
        jnp.bfloat16
    )
    dense_out = lax.psum_scatter(
        jnp.dot(dense_act, dense_down, preferred_element_type=jnp.float32).astype(jnp.bfloat16),
        "ep",
        scatter_dimension=0,
        tiled=True,
    ).astype(jnp.float32)
    new_hidden = (
        summed.astype(jnp.float32) + expert_sum + jax.nn.sigmoid(branch_gate)[None, :] * dense_out
    ).astype(jnp.bfloat16)
    return (new_hidden, new_lru, window[:, 1:])


def solution(mesh):
    in_specs = (
        P("ep", None),
        P(),
        P("ep", "tp"),
        P("ep", "tp"),
        P(None, "tp"),
        P("tp", None, None),
        P("tp", None, None),
        P("tp"),
        P("tp", None),
        P("ep", None, "tp"),
        P("ep", "tp"),
        P(),
        P("ep", None),
        P("ep", None),
        P("ep", None, "tp"),
        P("ep", None, "tp"),
        P("ep", "tp", None),
        P("tp", "ep"),
        P("tp", "ep"),
        P("ep", "tp"),
        P("tp"),
    )
    out_specs = (P("ep", "tp"), P("ep", "tp"), P("ep", None, "tp"))
    return jax.shard_map(
        on_device, mesh=mesh, in_specs=in_specs, out_specs=out_specs, check_vma=False
    )
```

profile of v0, /device:TPU:0, one launch (start us, length us, event | category | flops | bytes accessed | tf_op | source)
XLA Modules:
  0.0 329.7 jit_solution(14758161610007056048)
XLA Ops:
  7.2 0.0 copy-start
  7.2 0.0 reduce-scatter.5.cloned.1.call-start
  7.2 0.8 convert_element_type.111
  8.1 1.2 fusion.47
  9.2 1.1 fusion.49
  10.4 16.2 %all_to_all.29 = bf16[64,8,256]{2,0,1:T(8,128)(2,1)S(1)} all-to-all(bf16[64,8,256]{2,0,1:T(8,128)(2,1)S(1)} %bitcast.85), channel_id=1, replica_groups=mesh['ep'=8,'tp'=4] {'ep'}, dimensions={1} | all-to-all | bytes 524288 | tf_op jit(solution)/shard_map/all_to_all | solution.py:46
  26.6 2.5 convolution_convert_fusion.3
  29.0 0.0 reduce-scatter.5.cloned.1.call-update
  29.1 0.0 reduce-scatter.7.cloned.1.call-start
  29.2 0.1 copy.72
  29.3 0.1 eq.35
  29.4 62.9 %reduce-scatter.5.cloned.1.call-done = bf16[64,1024]{1,0:T(8,128)(2,1)} async-done(((bf16[512,1024]{1,0:T(8,128)(2,1)}), bf16[64,1024]{1,0:T(8,128)(2,1)}) %reduce-scatter.5.cloned.1.call-update) | async-done | bytes 131088 | tf_op jit(solution)/shard_map/reduce_scatter | solution.py:48
  92.3 0.8 slice_bitcast_fusion
  93.2 0.1 multiply_reduce_fusion
  93.2 0.1 convert_element_type.117
  93.4 0.4 copy-done.4
  93.8 0.7 copy-done.6
  94.5 1.1 fusion.38
  95.6 0.2 copy.69
  95.7 0.8 div.31
  96.5 1.2 fusion.34
  97.7 0.2 copy.71
  97.9 0.8 div.33
  98.6 1.1 multiply_add_fusion
  99.8 0.6 copy-done.5
  100.4 2.8 convolution_convert_fusion.2
  103.3 0.0 reduce-scatter.7.cloned.1.call-update
  103.3 0.1 fusion.71
  103.4 0.2 reduce_window_sum.11
  103.5 0.2 select_reduce_fusion
  103.7 18.8 %reduce-scatter.7.cloned.1.call-done = bf16[64,512]{1,0:T(8,128)(2,1)} async-done(((bf16[64,2048]{1,0:T(8,128)(2,1)}), bf16[64,512]{1,0:T(8,128)(2,1)}) %reduce-scatter.7.cloned.1.call-update) | async-done | bytes 65552 | tf_op jit(solution)/shard_map/reduce_scatter | solution.py:79
  122.6 0.9 add_convert_fusion
  123.5 0.6 copy-done.3
  124.1 5.8 %all_gather.6 = bf16[64,2048]{1,0:T(8,128)(2,1)S(1)} all-gather(bf16[64,512]{1,0:T(8,128)(2,1)S(1)} %add_convert_fusion), channel_id=1, replica_groups=mesh['ep'=8,'tp'=4] {'tp'}, dimensions={1}, use_global_device_ids=true | all-gather | bytes 327680 | tf_op jit(solution)/shard_map/all_gather | solution.py:84
  129.9 0.2 fusion.50
  130.0 0.1 fusion.52
  130.2 1.1 broadcast_in_dim.5
  131.3 2.0 reshape.106
  133.3 2.3 convolution_convert_fusion.1
  135.6 2.1 reshape.107
  137.7 5.5 %all-to-all-start.1 = ((bf16[8,18,2048]{2,1,0:T(8,128)(2,1)}), bf16[8,18,2048]{2,1,0:T(8,128)(2,1)}, u32[]{:S(2)}, u32[]{:S(2)}) async-start(bf16[8,18,2048]{2,1,0:T(8,128)(2,1)} %reshape.107), calls=%async_computation.3 | async-start | bytes 1572864 | tf_op jit(solution)/shard_map/all_to_all | solution.py:105
  143.2 0.0 all-reduce.2.cloned.1.call-start
  143.3 43.0 %all_gather.7 = bf16[512,512]{1,0:T(8,128)(2,1)S(1)} all-gather(bf16[64,512]{1,0:T(8,128)(2,1)S(1)} %constant_dynamic-slice_fusion), channel_id=1, replica_groups=mesh['ep'=8,'tp'=4] {'ep'}, dimensions={0}, use_global_device_ids=true | all-gather | bytes 589824 | tf_op jit(solution)/shard_map/all_gather | solution.py:131
  186.3 3.5 %convolution_convert_fusion = bf16[512,1536]{1,0:T(8,128)(2,1)} fusion(bf16[512,512]{1,0:T(8,128)(2,1)S(1)} %all_gather.7, bf16[512,768]{1,0:T(8,128)(2,1)} %param.39, bf16[512,768]{1,0:T(8,128)(2,1)} %param.38), kind=kOutput, calls=%fused_computation.6 | convolution fusion | flops 809238528 | bytes 3670016 | tf_op jit(solution)/shard_map/dot_general | solution.py:130
  189.8 0.0 all-reduce.2.cloned.1.call-update
  189.8 0.0 reduce-scatter.9.cloned.1.call-start
  189.9 3.8 %fusion.16 = f32[8,1,18,768]{3,2,0,1:T(8,128)} fusion(bf16[8,18,2048]{2,1,0:T(8,128)(2,1)} %all-to-all-done.1, bf16[1,2048,768]{2,1,0:T(8,128)(2,1)} %param.35), kind=kOutput, calls=%fused_computation.18 | convolution fusion | flops 452984832 | bytes 4177920 | tf_op jit(solution)/shard_map/sgid,gdf->sgif/dot_general | solution.py:108
  193.7 4.8 %fusion.9 = bf16[8,1,18,2048]{3,2,0,1:T(8,128)(2,1)} fusion(bf16[1,768,2048]{2,1,0:T(8,128)(2,1)S(1)} %copy-done, bf16[8,18,2048]{2,1,0:T(8,128)(2,1)} %all-to-all-done.1, bf16[1,2048,768]{2,1,0:T(8,128)(2,1)} %param.36, f32[8,1,18,768]{3,2,0,1:T(8,128)} %fusion.16), kind=kOutput, calls=%fused_computation.9 | convolution fusion | flops 906928128 | bytes 7913472 | tf_op jit(solution)/shard_map/sgif,gfd->sgid/dot_general | solution.py:113
  198.5 0.0 reduce-scatter.9.cloned.1.call-update
  198.5 0.0 reduce-scatter.11.cloned.1.call-start
  198.6 31.3 %all-reduce.2.cloned.1.call-done = bf16[512,1536]{1,0:T(8,128)(2,1)} async-done(((bf16[512,1536]{1,0:T(8,128)(2,1)}), bf16[512,1536]{1,0:T(8,128)(2,1)}) %all-reduce.2.cloned.1.call-update) | async-done | bytes 1572880 | tf_op jit(solution)/shard_map/psum | solution.py:135
  229.9 1.9 convert_element_type.138
  231.9 1.4 convolution_convert_fusion.4
  233.2 0.0 reduce-scatter.11.cloned.1.call-update
  233.3 0.1 reduce_sum.50
  233.4 0.1 copy.73
  233.5 22.1 %reduce-scatter.9.cloned.1.call-done = bf16[8,1,18,512]{3,2,0,1:T(8,128)(2,1)} async-done(((bf16[8,1,18,2048]{3,2,0,1:T(8,128)(2,1)}), bf16[8,1,18,512]{3,2,0,1:T(8,128)(2,1)}) %reduce-scatter.9.cloned.1.call-update) | async-done | bytes 147472 | tf_op jit(solution)/shard_map/reduce_scatter | solution.py:116
  255.6 5.5 %all-to-all-start.2 = ((bf16[8,18,512]{2,1,0:T(8,128)(2,1)}), bf16[8,18,512]{2,1,0:T(8,128)(2,1)S(1)}, u32[]{:S(2)}, u32[]{:S(2)}) async-start(bf16[8,18,512]{2,1,0:T(8,128)(2,1)} %bitcast.86), calls=%async_computation.5 | async-start | bytes 393216 | tf_op jit(solution)/shard_map/all_to_all | solution.py:120
  261.1 0.7 multiply_reduce_fusion.1
  261.9 1.5 fusion.57
  263.4 5.6 %all-to-all-done.2 = bf16[8,18,512]{2,1,0:T(8,128)(2,1)S(1)} async-done(((bf16[8,18,512]{2,1,0:T(8,128)(2,1)}), bf16[8,18,512]{2,1,0:T(8,128)(2,1)S(1)}, u32[]{:S(2)}, u32[]{:S(2)}) %all-to-all-start.2) | async-done | bytes 147488 | tf_op jit(solution)/shard_map/all_to_all | solution.py:120
  269.0 0.1 reshape.113
  269.0 52.4 %reduce-scatter.11.cloned.1.call-done = bf16[64,512]{1,0:T(8,128)(2,1)} async-done(((bf16[512,512]{1,0:T(8,128)(2,1)}), bf16[64,512]{1,0:T(8,128)(2,1)}) %reduce-scatter.11.cloned.1.call-update) | async-done | bytes 65552 | tf_op jit(solution)/shard_map/reduce_scatter | solution.py:139
  321.5 1.7 fusion.40
  (34 shorter events, 0.2 us)
Async XLA Ops:
  7.2 186.5 %copy-start = (bf16[1,768,2048]{2,1,0:T(8,128)(2,1)S(1)}, bf16[1,768,2048]{2,1,0:T(8,128)(2,1)}, u32[]{:S(2)}) copy-start(bf16[1,768,2048]{2,1,0:T(8,128)(2,1)} %param.37) | copy-start | bytes 9437188
  7.2 85.2 %reduce-scatter.5.cloned.1.call-start = ((), (), s32[]{:S(2)}) async-start(), calls=%async_computation.7 | async-start | bytes 1179648 | tf_op jit(solution)/shard_map/reduce_scatter | solution.py:48
  10.3 18.8 %copy-start.7 = (bf16[4,512]{1,0:T(4,128)(2,1)S(1)}, bf16[4,512]{1,0:T(4,128)(2,1)}, u32[]{:S(2)}) copy-start(bf16[4,512]{1,0:T(4,128)(2,1)} %param.25) | copy-start | bytes 12292
  10.4 18.8 %copy-start.8 = (bf16[2048]{0:T(1024)(128)(2,1)S(1)}, bf16[2048]{0:T(1024)(128)(2,1)}, u32[]{:S(2)}) copy-start(bf16[2048]{0:T(1024)(128)(2,1)} %param.32) | copy-start | bytes 12292
  10.4 18.8 %copy-start.9 = (s32[64,2]{0,1:T(2,128)S(1)}, s32[64,2]{0,1:T(2,128)}, u32[]{:S(2)}) copy-start(s32[64,2]{0,1:T(2,128)} %param.33) | copy-start | bytes 1540
  10.4 19.0 %copy-start.10 = (f32[512]{0:T(512)S(1)}, f32[512]{0:T(512)}, u32[]{:S(2)}) copy-start(f32[512]{0:T(512)} %param.28) | copy-start | bytes 6148
  10.4 82.8 %copy-start.1 = (bf16[64,3,512]{2,0,1:T(8,128)(2,1)S(1)}, bf16[64,3,512]{2,0,1:T(8,128)(2,1)}, u32[]{:S(2)}) copy-start(bf16[64,3,512]{2,0,1:T(8,128)(2,1)} %param.30) | copy-start | bytes 589828
  29.1 93.5 %reduce-scatter.7.cloned.1.call-start = ((), (), s32[]{:S(2)}) async-start(), calls=%async_computation.8 | async-start | bytes 327680 | tf_op jit(solution)/shard_map/reduce_scatter | solution.py:79
  93.2 0.6 copy-start.4
  93.8 0.7 copy-start.6
  99.8 0.7 copy-start.5
  123.5 0.6 copy-start.3
  137.7 52.2 %all-to-all-start.1 = ((bf16[8,18,2048]{2,1,0:T(8,128)(2,1)}), bf16[8,18,2048]{2,1,0:T(8,128)(2,1)}, u32[]{:S(2)}, u32[]{:S(2)}) async-start(bf16[8,18,2048]{2,1,0:T(8,128)(2,1)} %reshape.107), calls=%async_computation.3 | async-start | bytes 1572864 | tf_op jit(solution)/shard_map/all_to_all | solution.py:105
  143.2 86.7 %all-reduce.2.cloned.1.call-start = ((), (), s32[]{:S(2)}) async-start(), calls=%async_computation.10 | async-start | bytes 3145728 | tf_op jit(solution)/shard_map/psum | solution.py:135
  189.8 65.8 %reduce-scatter.9.cloned.1.call-start = ((), (), s32[]{:S(2)}) async-start(), calls=%async_computation.9 | async-start | bytes 983040 | tf_op jit(solution)/shard_map/reduce_scatter | solution.py:116
  198.5 122.9 %reduce-scatter.11.cloned.1.call-start = ((), (), s32[]{:S(2)}) async-start(), calls=%async_computation.11 | async-start | bytes 589824 | tf_op jit(solution)/shard_map/reduce_scatter | solution.py:139
  229.9 1.9 copy-start.13
  231.8 1.7 copy-start.11
  231.8 29.3 %copy-start.12 = (f32[64,2]{0,1:T(2,128)S(1)}, f32[64,2]{0,1:T(2,128)}, u32[]{:S(2)}) copy-start(f32[64,2]{0,1:T(2,128)} %param.34) | copy-start | bytes 1540
  231.8 30.0 %copy-start.2 = (bf16[64,3,512]{2,0,1:T(8,128)(2,1)S(1)}, bf16[64,3,512]{2,0,1:T(8,128)(2,1)}, u32[]{:S(2)}) copy-start(bf16[64,3,512]{2,0,1:T(8,128)(2,1)} %param.30) | copy-start | bytes 589828
  255.6 13.4 %all-to-all-start.2 = ((bf16[8,18,512]{2,1,0:T(8,128)(2,1)}), bf16[8,18,512]{2,1,0:T(8,128)(2,1)S(1)}, u32[]{:S(2)}, u32[]{:S(2)}) async-start(bf16[8,18,512]{2,1,0:T(8,128)(2,1)} %bitcast.86), calls=%async_computation.5 | async-start | bytes 393216 | tf_op jit(solution)/shard_map/all_to_all | solution.py:120
Sparse Core Ops, SparseCore 0:
  29.2 63.1 reduce-scatter.4
  103.4 19.1 reduce-scatter.6
  190.0 39.9 all-reduce.1
  232.3 23.2 reduce-scatter.8
  258.8 62.6 reduce-scatter.10
where the time goes:
time: 331 us; the launch traced here: 330 us
  waiting for transfers between devices  193 us (58%)
  blocking collectives  64.9 us (20%)
  matrix products  25.1 us (8%)
  between operations  14.1 us (4%)
  starting transfers between devices  11.2 us (3%)
  local copies, waits for them, and re-layouts  11 us (3%)
  other arithmetic  10.1 us (3%)
    reduce_scatter x1, waiting for transfers between devices, on_device(): lax.psum_scatter(jnp.dot(spread, weights_xy, preferred_element_type=jnp.f...  62.9 us
    reduce_scatter x1, waiting for transfers between devices, on_device(): lax.psum_scatter(jnp.dot(dense_act, dense_down, preferred_element_type=jn...  52.4 us
    all_gather x1, blocking collectives, on_device(): lax.all_gather(ffn_cols, 'ep', axis=0, tiled=True)  43 us
    psum x1, waiting for transfers between devices, on_device(): lax.psum(dense_part.astype(jnp.bfloat16), 'tp').astype(jnp.float32)  31.3 us
    reduce_scatter x1, waiting for transfers between devices, on_device(): lax.psum_scatter(partial_out.astype(jnp.bfloat16), 'tp', scatter_dimensio...  22.1 us
    reduce_scatter x1, waiting for transfers between devices, on_device(): lax.psum_scatter(partial_value.astype(jnp.bfloat16), 'tp', scatter_dimens...  18.8 us
    all_to_all x1, blocking collectives, on_device(): lax.all_to_all(normed, 'ep', split_axis=1, concat_axis=0, tiled=True)  16.2 us
  transfers between devices with their start and end apart: 7, of which 6 were waited for; matrix products, arithmetic and copies ran while one was open for 6% of the time, Pallas kernels for 0%

commit v1 on v0

v1 whole, which is shorter than its diff:
```python
import functools

import jax
import jax.numpy as jnp
from jax import lax
from jax.experimental import pallas as pl
from jax.experimental.pallas import tpu as pltpu
from jax.sharding import PartitionSpec as P

epsilon = 1e-06
decay_scale = 8.0
MESH = pl.DeviceIdType.MESH
F32 = jnp.float32
BF16 = jnp.bfloat16


def rms_scale(values, gain_vec):
    floats = values.astype(F32)
    meansq = jnp.mean(floats * floats, axis=-1, keepdims=True)
    return floats * lax.rsqrt(meansq + epsilon) * gain_vec.astype(F32)


def dot(a, b):
    return jnp.dot(a, b, preferred_element_type=F32)


def layer_kernel(
    E, T, slots,
    nb, ct, hid_own, wx, wy, conv_pre, tap_new, bd, log_dec, lru, gain_own, branch,
    po_h, dwp_h, eg_h, eu_h, ed_h, dd_h,
    new_hidden, new_lru, x_out,
    po, eg, eu, ed, dd, dwr, spread, pbuf, parts, ctr, acc, mbuf, mrec, qbuf, qrec,
    xall, hacc, aall, xe, hid, sel, ebuf, erec, obuf, orec, summed_ref,
    load_sem, nb_s, nb_r, ct_s, ct_r, pt_s, pt_r, dw_s, dw_r, mx_s, mx_r, q_s, q_r,
    xe_s, x2_s, x1_s, x_r, a_s, a_r, er_s, er_r, o_s, o_r,
):
    e = lax.axis_index("ep")
    t = lax.axis_index("tp")
    M, C = hid_own.shape
    D = C * T

    def ep_peer(k):
        return lax.rem(e + k, E)

    def ep_from(k):
        return lax.rem(e + E - k, E)

    def tp_peer(k):
        return lax.rem(t + k, T)

    across = lax.rem(t + T // 2, T)
    beside = t + 1 - 2 * lax.rem(t, 2)
    diagonal = lax.rem(beside + T // 2, T)

    loads = [
        pltpu.make_async_copy(src, dst, load_sem.at[i])
        for i, (src, dst) in enumerate(
            ((po_h, po), (eg_h, eg), (eu_h, eu), (ed_h, ed), (dd_h, dd))
        )
    ]
    own_dw = pltpu.make_async_copy(dwp_h.at[t], dwr.at[t], load_sem.at[5])

    def rcopy(src, dst, s, r, ep=None, tp=None):
        return pltpu.make_async_remote_copy(
            src_ref=src, dst_ref=dst, send_sem=s, recv_sem=r,
            device_id=(e if ep is None else ep, t if tp is None else tp),
            device_id_type=MESH,
        )

    barrier = pltpu.get_barrier_semaphore()

    @pl.loop(1, E)
    def _(k):
        pl.semaphore_signal(barrier, inc=1, device_id=(ep_peer(k), t), device_id_type=MESH)

    for k in range(1, T):
        pl.semaphore_signal(barrier, inc=1, device_id=(e, tp_peer(k)), device_id_type=MESH)
    pl.semaphore_wait(barrier, E - 1 + T - 1)

    @pl.loop(1, E)
    def _(k):
        p = ep_peer(k)
        rcopy(nb.at[p], spread.at[e], nb_s.at[p], nb_r.at[e], ep=p).start()
        rcopy(ct.at[p], ctr.at[e], ct_s.at[p], ct_r.at[e], ep=p).start()

    loads[0].start()
    own_dw.start()
    for k in range(1, T):
        j = tp_peer(k)
        rcopy(dwp_h.at[j], dwr.at[t], dw_s.at[j], dw_r.at[t], tp=j).start()
    for l in loads[1:]:
        l.start()

    acc[:, :C] = dot(nb[e], wx[...])
    acc[:, C:] = dot(nb[e], wy[...])

    @pl.loop(1, E)
    def _(k):
        s = ep_from(k)
        rcopy(nb.at[s], spread.at[s], nb_s.at[s], nb_r.at[s], ep=s).wait_recv()
        blk = spread[s]
        pbuf[s, :, :C] = dot(blk, wx[...]).astype(BF16)
        pbuf[s, :, C:] = dot(blk, wy[...]).astype(BF16)
        rcopy(pbuf.at[s], parts.at[e], pt_s.at[s], pt_r.at[e], ep=s).start()

    @pl.loop(1, E)
    def _(k):
        s = ep_from(k)
        rcopy(ct.at[s], ctr.at[s], ct_s.at[s], ct_r.at[s], ep=s).wait_recv()

    ctr[e] = ct[e]
    N = E * M
    w_row = ctr[0]
    for s in range(1, E):
        w_row = w_row + ctr[s]
    nblk = min(N, 512)
    tri = (
        lax.broadcasted_iota(jnp.int32, (nblk, nblk), 0)
        < lax.broadcasted_iota(jnp.int32, (nblk, nblk), 1)
    ).astype(F32).astype(BF16)
    base = jnp.zeros((1, 1), F32)
    w_slot = jnp.zeros((slots, 1), F32)
    for b in range(N // nblk):
        w_b = w_row[:, b * nblk:(b + 1) * nblk]
        m_b = (w_b > 0.0).astype(F32)
        rank = dot(jnp.broadcast_to(m_b, (16, nblk)).astype(BF16), tri)[0:1, :] + base
        base = base + jnp.sum(m_b, axis=1, keepdims=True)
        hit = (
            lax.broadcasted_iota(jnp.int32, (slots, nblk), 0).astype(F32) == rank
        ).astype(F32) * m_b
        sel[:, b * nblk:(b + 1) * nblk] = hit.astype(BF16)
        w_slot = w_slot + jnp.sum(hit * w_b, axis=1, keepdims=True)

    @pl.loop(1, E)
    def _(k):
        p = ep_peer(k)
        rcopy(pbuf.at[p], parts.at[p], pt_s.at[p], pt_r.at[p], ep=p).wait_recv()
        acc[...] += parts[p].astype(F32)

    x_b = acc[:, :C].astype(BF16)
    y_b = acc[:, C:].astype(BF16)
    x_out[...] = x_b
    conv = (conv_pre[...] + x_b.astype(F32) * tap_new[...]).astype(BF16)
    width = bd.shape[1]
    gi, gd = [], []
    for i in range(C // width):
        g = dot(conv[:, i * width:(i + 1) * width], bd[i])
        gi.append(g[:, :width])
        gd.append(g[:, width:])
    gate_in = jax.nn.sigmoid(jnp.concatenate(gi, axis=1))
    gate_dec = jax.nn.sigmoid(jnp.concatenate(gd, axis=1))
    log_decay = gate_dec * log_dec[...]
    decay = jnp.exp(log_decay)
    inject = jnp.sqrt(-jnp.tanh(log_decay) * (1.0 + decay * decay))
    state = decay * lru[...] + inject * gate_in * conv.astype(F32)
    new_lru[...] = state
    gated = (state * jax.nn.gelu(y_b.astype(F32), approximate=True)).astype(BF16)

    loads[0].wait()
    order = [tp_peer(k) for k in (2, 3, 1)] if T == 4 else [tp_peer(k) for k in range(1, T)]
    for j in order:
        cols = pl.ds(pl.multiple_of(j * C, 128), C)
        mbuf[j] = dot(gated, po[:, cols]).astype(BF16)
        rcopy(mbuf.at[j], mrec.at[t], mx_s.at[j], mx_r.at[t], tp=j).start()
    own_cols = pl.ds(pl.multiple_of(t * C, 128), C)
    mixer = dot(gated, po[:, own_cols]).astype(BF16).astype(F32)
    for j in reversed(order):
        rcopy(mbuf.at[j], mrec.at[j], mx_s.at[j], mx_r.at[j], tp=j).wait_recv()
        mixer = mixer + mrec[j].astype(F32)
    summed = (hid_own[...].astype(F32) + mixer).astype(BF16)
    summed_ref[...] = summed
    sf = summed.astype(F32)
    ssq = jnp.sum(sf * sf, axis=1, keepdims=True)
    qbuf[...] = jnp.broadcast_to(ssq, qbuf.shape)
    for j in order:
        rcopy(qbuf, qrec.at[t], q_s.at[j], q_r.at[t], tp=j).start()
    total = qbuf[...]
    for j in reversed(order):
        rcopy(qbuf, qrec.at[j], q_s.at[j], q_r.at[j], tp=j).wait_recv()
        total = total + qrec[j]
    scale = lax.rsqrt(total[:, 0:1] * (1.0 / D) + epsilon)
    xall[t, e] = (sf * scale * gain_own[...]).astype(BF16)

    @pl.loop(1, E)
    def _(k):
        p = ep_peer(k)
        rcopy(xall.at[t, e], xall.at[t, e], xe_s.at[p], x_r.at[t, e], ep=p).start()

    def spread_tp(s):
        rcopy(xall.at[t, s], xall.at[t, s], x2_s.at[s], x_r.at[t, s], tp=across).start()
        rcopy(xall.at[t, s], xall.at[t, s], x1_s.at[0, s], x_r.at[t, s], tp=beside).start()

    def forward(s):
        rcopy(xall.at[across, s], xall.at[across, s], x2_s.at[s], x_r.at[across, s], tp=across).wait_recv()
        rcopy(xall.at[across, s], xall.at[across, s], x1_s.at[1, s], x_r.at[across, s], tp=beside).start()

    spread_tp(e)

    @pl.loop(1, E)
    def _(k):
        s = ep_from(k)
        rcopy(xall.at[t, s], xall.at[t, s], xe_s.at[s], x_r.at[t, s], ep=s).wait_recv()
        spread_tp(s)
        forward(ep_from(k - 1))

    forward(ep_from(E - 1))

    @pl.loop(0, E)
    def _(s):
        rcopy(xall.at[beside, s], xall.at[beside, s], x1_s.at[0, s], x_r.at[beside, s], tp=beside).wait_recv()
        rcopy(xall.at[diagonal, s], xall.at[diagonal, s], x1_s.at[1, s], x_r.at[diagonal, s], tp=beside).wait_recv()

    own_dw.wait()
    for j in order:
        rcopy(dwp_h.at[j], dwr.at[j], dw_s.at[j], dw_r.at[j], tp=j).wait_recv()
    rows = min(N, 512)

    @pl.loop(0, N // rows)
    def _(b):
        hacc[...] = jnp.zeros_like(hacc)
        eb = rows // M

        @pl.loop(0, T)
        def _(q):
            xq = xall[q, pl.ds(b * eb, eb)].reshape(rows, C)
            hacc[...] += dot(xq, dwr[q])

        h = hacc[...]
        half = h.shape[1] // 2
        act = jax.nn.silu(h) * pltpu.roll(h, half, axis=1)
        aall[t, pl.ds(pl.multiple_of(b * rows, 16), rows), :] = act[:, :half].astype(BF16)

    a_across = rcopy(aall.at[t], aall.at[t], a_s.at[0], a_r.at[t], tp=across)
    a_beside = rcopy(aall.at[t], aall.at[t], a_s.at[1], a_r.at[t], tp=beside)
    a_across.start()
    a_beside.start()

    @pl.loop(0, T)
    def _(q):
        cols = pl.ds(pl.multiple_of(q * C, 128), C)
        xe[:, cols] = dot(sel[...], xall[q].reshape(N, C)).astype(BF16)

    loads[1].wait()
    loads[2].wait()
    FH = eg.shape[1]
    nch = 256 if FH % 256 == 0 else FH

    @pl.loop(0, FH // nch)
    def _(n):
        cols = pl.ds(pl.multiple_of(n * nch, 128), nch)
        g = dot(xe[...], eg[:, cols])
        u = dot(xe[...], eu[:, cols])
        hid[:, cols] = (jax.nn.silu(g) * u).astype(BF16)

    a_in = rcopy(aall.at[across], aall.at[across], a_s.at[0], a_r.at[across], tp=across)
    a_in.wait_recv()
    a_fwd = rcopy(aall.at[across], aall.at[across], a_s.at[2], a_r.at[across], tp=beside)
    a_fwd.start()

    loads[3].wait()
    for j in order:
        cols = pl.ds(pl.multiple_of(j * C, 128), C)
        ebuf[j] = dot(hid[...], ed[:, cols]).astype(BF16)
        rcopy(ebuf.at[j], erec.at[t], er_s.at[j], er_r.at[t], tp=j).start()
    ebuf[t] = dot(hid[...], ed[:, own_cols]).astype(BF16)

    loads[4].wait()
    rcopy(aall.at[beside], aall.at[beside], a_s.at[1], a_r.at[beside], tp=beside).wait_recv()
    rcopy(aall.at[diagonal], aall.at[diagonal], a_s.at[2], a_r.at[diagonal], tp=beside).wait_recv()
    red = ebuf[t].astype(F32)
    for j in reversed(order):
        rcopy(ebuf.at[j], erec.at[j], er_s.at[j], er_r.at[j], tp=j).wait_recv()
        red = red + erec[j].astype(F32)
    red = (red.astype(BF16).astype(F32) * w_slot).astype(BF16)
    gate = jax.nn.sigmoid(branch[...])
    ob = 128 if N % 128 == 0 else M
    ebuf[t] = red

    @pl.loop(0, N // ob)
    def _(b):
        rws = pl.ds(pl.multiple_of(b * ob, 128 if ob % 128 == 0 else 16), ob)
        d = dot(aall[0, rws, :], dd[0])
        for q in range(1, T):
            d = d + dot(aall[q, rws, :], dd[q])
        d = d * gate + lax.dot_general(
            sel[:, rws], ebuf[t], (((0,), (0,)), ((), ())), preferred_element_type=F32
        )
        obuf[pl.ds(b * (ob // M), ob // M)] = d.reshape(ob // M, M, C).astype(BF16)

    @pl.loop(1, E)
    def _(k):
        p = ep_peer(k)
        rcopy(obuf.at[p], orec.at[e], o_s.at[p], o_r.at[e], ep=p).start()

    acc[:, :C] = summed_ref[...].astype(F32) + obuf[e].astype(F32)

    @pl.loop(1, E)
    def _(k):
        s = ep_from(k)
        rcopy(obuf.at[s], orec.at[s], o_s.at[s], o_r.at[s], ep=s).wait_recv()
        acc[:, :C] += orec[s].astype(F32)

    new_hidden[...] = acc[:, :C].astype(BF16)

    @pl.loop(1, E)
    def _(k):
        p = ep_peer(k)
        rcopy(nb.at[p], spread.at[e], nb_s.at[p], nb_r.at[e], ep=p).wait_send()
        rcopy(ct.at[p], ctr.at[e], ct_s.at[p], ct_r.at[e], ep=p).wait_send()
        rcopy(pbuf.at[p], parts.at[e], pt_s.at[p], pt_r.at[e], ep=p).wait_send()
        rcopy(xall.at[t, e], xall.at[t, e], xe_s.at[p], x_r.at[t, e], ep=p).wait_send()
        rcopy(obuf.at[p], orec.at[e], o_s.at[p], o_r.at[e], ep=p).wait_send()

    for j in order:
        rcopy(dwp_h.at[j], dwr.at[t], dw_s.at[j], dw_r.at[t], tp=j).wait_send()
        rcopy(mbuf.at[j], mrec.at[t], mx_s.at[j], mx_r.at[t], tp=j).wait_send()
        rcopy(qbuf, qrec.at[t], q_s.at[j], q_r.at[t], tp=j).wait_send()
        rcopy(ebuf.at[j], erec.at[t], er_s.at[j], er_r.at[t], tp=j).wait_send()

    @pl.loop(0, E)
    def _(s):
        rcopy(xall.at[t, s], xall.at[t, s], x2_s.at[s], x_r.at[t, s], tp=across).wait_send()
        rcopy(xall.at[t, s], xall.at[t, s], x1_s.at[0, s], x_r.at[t, s], tp=beside).wait_send()
        rcopy(xall.at[across, s], xall.at[across, s], x1_s.at[1, s], x_r.at[across, s], tp=beside).wait_send()

    a_across.wait_send()
    a_beside.wait_send()
    a_fwd.wait_send()


def on_device(
    hidden, mix_gain, proj_x, proj_y, conv_taps, input_gate, decay_gate, decay_param,
    proj_out, conv_state, lru_state, ffn_gain, routes, route_weights,
    expert_gate, expert_up, expert_down, dense_gate, dense_up, dense_down, branch_gate,
):
    E = lax.axis_size("ep")
    T = lax.axis_size("tp")
    e = lax.axis_index("ep")
    t = lax.axis_index("tp")
    M, D = hidden.shape
    C = D // T
    R = proj_x.shape[0]
    N = E * M
    normed = rms_scale(hidden, mix_gain).astype(BF16)
    nb = normed.reshape(M, E, R).transpose(1, 0, 2)
    hid_own = lax.dynamic_slice_in_dim(hidden, t * C, C, 1)
    gain_own = lax.dynamic_slice_in_dim(ffn_gain, t * C, C, 0).astype(F32)[None, :]
    taps = conv_taps.astype(F32)
    conv_pre = jnp.sum(conv_state.astype(F32) * taps[None, :-1], axis=1)
    heads, block = input_gate.shape[:2]
    group = max(1, 128 // block)

    def diag(g):
        g = g.reshape(heads // group, group, block, 1, block)
        eye = jnp.eye(group, dtype=g.dtype).reshape(1, group, 1, group, 1)
        return (g * eye).reshape(heads // group, group * block, group * block)

    bd = jnp.concatenate([diag(input_gate), diag(decay_gate)], axis=2)
    log_dec = (decay_scale * jax.nn.log_sigmoid(decay_param))[None, :]
    experts = expert_gate.shape[0] * E
    ids = jnp.arange(experts, dtype=jnp.int32)
    rows_w = jnp.sum(
        jnp.where(routes.T[None, :, :] == ids[:, None, None], route_weights.T[None], 0.0), axis=1
    )
    here = (jnp.arange(E) == e).astype(F32)
    ct = (here[None, :, None] * rows_w[:, None, :]).reshape(experts, 1, N)
    capacity = M * routes.shape[1] // experts + 2
    slots = -(-E * capacity // 16) * 16
    h = dense_gate.shape[1] // T
    half = -(-2 * h // 128) * 64

    def cut(w):
        w = w.reshape(C, T, h).transpose(1, 0, 2)
        return jnp.pad(w, ((0, 0), (0, 0), (0, half - h)))

    dwp = jnp.concatenate([cut(dense_gate), cut(dense_up)], axis=2)
    dd = jnp.pad(dense_down.reshape(T, h, C), ((0, 0), (0, half - h), (0, 0)))
    FH = expert_gate.shape[2]
    vm = pl.BlockSpec(memory_space=pltpu.VMEM)
    anyspace = pl.BlockSpec(memory_space=pl.ANY)
    DMA = pltpu.SemaphoreType.DMA
    V = pltpu.VMEM
    rows = min(N, 512)
    scratch = [
        V((C, D), BF16), V((D, FH), BF16), V((D, FH), BF16), V((FH, D), BF16), V((T, half, C), BF16),
        V((T, C, 2 * half), BF16),
        V((E, M, R), BF16), V((E, M, 2 * C), BF16), V((E, M, 2 * C), BF16), V((E, 1, N), F32),
        V((M, 2 * C), F32),
        V((T, M, C), BF16), V((T, M, C), BF16), V((M, 128), F32), V((T, M, 128), F32),
        V((T, E, M, C), BF16), V((rows, 2 * half), F32), V((T, N, half), BF16),
        V((slots, D), BF16), V((slots, FH), BF16), V((slots, N), BF16),
        V((T, slots, C), BF16), V((T, slots, C), BF16), V((E, M, C), BF16), V((E, M, C), BF16),
        V((M, C), BF16),
        DMA((6,)),
        DMA((E,)), DMA((E,)), DMA((E,)), DMA((E,)), DMA((E,)), DMA((E,)),
        DMA((T,)), DMA((T,)), DMA((T,)), DMA((T,)), DMA((T,)), DMA((T,)),
        DMA((E,)), DMA((E,)), DMA((2, E)), DMA((T, E)), DMA((3,)), DMA((T,)), DMA((T,)), DMA((T,)),
        DMA((E,)), DMA((E,)),
    ]
    new_hidden, new_lru, x_new = pl.pallas_call(
        functools.partial(layer_kernel, E, T, slots),
        out_shape=(
            jax.ShapeDtypeStruct((M, C), BF16),
            jax.ShapeDtypeStruct((M, C), F32),
            jax.ShapeDtypeStruct((M, C), BF16),
        ),
        in_specs=[vm] * 12 + [anyspace] * 6,
        out_specs=(vm, vm, vm),
        scratch_shapes=scratch,
        compiler_params=pltpu.CompilerParams(
            collective_id=0, has_side_effects=True, vmem_limit_bytes=60 * 1024 * 1024
        ),
    )(
        nb, ct, hid_own, proj_x, proj_y, conv_pre, taps[-1:], bd, log_dec, lru_state, gain_own,
        branch_gate[None, :], proj_out, dwp, expert_gate[0], expert_up[0], expert_down[0], dd,
    )
    new_conv = jnp.concatenate([conv_state[:, 1:], x_new[:, None, :]], axis=1)
    return (new_hidden, new_lru, new_conv)


def solution(mesh):
    in_specs = (
        P("ep", None),
        P(),
        P("ep", "tp"),
        P("ep", "tp"),
        P(None, "tp"),
        P("tp", None, None),
        P("tp", None, None),
        P("tp"),
        P("tp", None),
        P("ep", None, "tp"),
        P("ep", "tp"),
        P(),
        P("ep", None),
        P("ep", None),
        P("ep", None, "tp"),
        P("ep", None, "tp"),
        P("ep", "tp", None),
        P("tp", "ep"),
        P("tp", "ep"),
        P("ep", "tp"),
        P("tp"),
    )
    out_specs = (P("ep", "tp"), P("ep", "tp"), P("ep", None, "tp"))
    return jax.shard_map(
        on_device, mesh=mesh, in_specs=in_specs, out_specs=out_specs, check_vma=False
    )
```

time: 331 us -> 116 us (0.35)
  waiting for transfers between devices: 193 us -> 0 us
  Pallas kernels: 0 us -> 93.9 us
  blocking collectives: 64.9 us -> 0 us
  matrix products: 25.1 us -> 0 us
  between operations: 14.1 us -> 0.8 us
  starting transfers between devices: 11.2 us -> 0 us
    reduce_scatter x4 -> x0, waiting for transfers between devices: 156 us -> none  [the longest x1 62.9 us: on_device(): lax.psum_scatter(jnp.dot(spread, weights_xy, preferred_element_type=jnp.f...]
    pallas_call x0 -> x1, Pallas kernels: none -> 93.9 us  [on_device(): pl.pallas_call(functools.partial(layer_kernel, E, T, slots), out_shape=(j...]
    all_gather x2 -> x0, blocking collectives: 48.8 us -> none  [the longest x1 43 us: on_device(): lax.all_gather(ffn_cols, 'ep', axis=0, tiled=True)]
    psum x1 -> x0, waiting for transfers between devices: 31.3 us -> none  [on_device(): lax.psum(dense_part.astype(jnp.bfloat16), 'tp').astype(jnp.float32)]
    dot_general x10 -> x0, matrix products: 25.1 us -> none  [the longest x1 4.83 us: on_device(): jnp.einsum('sgif,gfd->sgid', inner_act, expert_down, preferred_element_ty...]
    all_to_all x1 -> x0, blocking collectives: 16.2 us -> none  [on_device(): lax.all_to_all(normed, 'ep', split_axis=1, concat_axis=0, tiled=True)]
    all_to_all x2 -> x0, starting transfers between devices: 11 us -> none  [the longest x1 5.52 us: on_device(): lax.all_to_all(dispatch, 'ep', split_axis=0, concat_axis=0, tiled=True)]
    all_to_all x2 -> x0, waiting for transfers between devices: 5.58 us -> none  [the longest x1 5.58 us: on_device(): lax.all_to_all(flat_back, 'ep', split_axis=0, concat_axis=0, tiled=True)]
  transfers between devices with their start and end apart: 7 -> 0, of which waited for: 6 -> 0; matrix products, arithmetic and copies ran while one was open for 6% -> 0% of each run, Pallas kernels for 0% -> 0%
where the time goes in v1:
time: 116 us; the launch traced here: 115 us
  Pallas kernels  93.9 us (81%)
  local copies, waits for them, and re-layouts  11.5 us (10%)
  other arithmetic  8.29 us (7%)
    pallas_call x1, Pallas kernels, on_device(): pl.pallas_call(functools.partial(layer_kernel, E, T, slots), out_shape=(j...  93.9 us
    unnamed x16, local copies, waits for them, and re-layouts  4.77 us
    mul x6, local copies, waits for them, and re-layouts, diag(): return (g * eye).reshape(heads // group, group * block, group * block)  2.63 us

profile of v1, /device:TPU:0, one launch (start us, length us, event | category | flops | bytes accessed | tf_op | source)
XLA Modules:
  0.0 114.6 jit_solution(6972910118612074656)
XLA Ops:
  0.6 0.0 copy-start.1
  0.6 1.5 %constant_dynamic-slice_fusion.hid_own = bf16[64,512]{1,0:T(8,128)(2,1)} fusion(bf16[64,2048]{1,0:T(8,128)(2,1)} %param.21, s32[]{:T(128)S(6)} %select_n.14), kind=kLoop, calls=%fused_computation.22 | loop fusion | bytes 131076 | tf_op jit(solution)/shard_map/dynamic_slice | solution.py:346
  2.2 1.3 %dynamic-slice_convert_fusion = f32[512]{0:T(512)} fusion(bf16[2048]{0:T(1024)(128)(2,1)} %param.32, s32[]{:T(128)S(6)} %select_n.14), kind=kLoop, calls=%fused_computation.20 | loop fusion | flops 512 | bytes 3076 | tf_op jit(solution)/shard_map/broadcast_in_dim | solution.py:347
  3.5 1.1 mul.122
  4.6 0.1 mul.123
  4.8 1.1 mul.129
  5.8 0.1 mul.130
  6.0 0.1 mul.124
  6.1 0.1 mul.125
  6.2 0.7 pad_maximum_fusion.1.bd
  7.0 0.1 mul.112
  7.0 0.1 mul.113
  7.1 0.7 select_reduce_fusion
  7.8 0.1 mul.116
  7.9 0.6 broadcast_multiply_fusion.2.ct
  8.5 0.0 copy-done.1
  8.6 0.3 copy.32
  8.8 0.5 copy.33
  9.4 1.4 %copy.30 = bf16[512,768]{0,1:T(8,128)(2,1)S(1)} copy(bf16[512,768]{1,0:T(8,128)(2,1)} %param.38) | data formatting | bytes 1572864 | tf_op args[17]
  10.8 0.0 copy-start.4
  10.8 0.0 copy-start
  10.8 0.0 copy-start.3
  10.8 0.0 copy-start.2
  10.8 0.0 copy-start.5
  10.8 0.5 copy.31
  11.3 1.7 %pad_maximum_fusion.dwp_h = bf16[4,512,384]{2,1,0:T(8,128)(2,1)} fusion(bf16[4,512,192]{2,1,0:T(8,128)(2,1)S(1)} %bitcast.23, bf16[4,512,192]{2,1,0:T(8,128)(2,1)S(1)} %bitcast.24), kind=kLoop, calls=%fused_computation | loop fusion | flops 3145728 | bytes 3145728 | tf_op jit(solution)/shard_map/concatenate | solution.py:376
  13.1 0.0 copy-done.4
  13.1 0.0 copy-done
  13.1 0.2 fusion
  13.3 0.1 fusion.2
  13.4 0.7 copy.36
  14.1 0.0 copy-done.3
  14.1 0.0 copy-done.2
  14.1 0.7 multiply_reduce_fusion.conv_pre
  14.8 0.0 copy-done.5
  14.8 0.6 fusion.4
  15.4 0.6 slice.13.tap_new
  16.0 0.0 slice-start
  16.0 93.9 %shard_map.220 = (bf16[64,512]{1,0:T(8,128)(2,1)}, f32[64,512]{1,0:T(8,128)}, bf16[64,512]{1,0:T(8,128)(2,1)}) custom-call(bf16[8,64,256]{2,1,0:T(8,128)(2,1)} %bitcast.30, f32[8,1,512]{2,1,0:T(1,128)} %broadcast_multiply_fusion.2.ct, bf16[64,512]{1,0:T(8,128)(2,1)} %constant_dynamic-slice_fusion.hid_own, bf16[256,512]{1,0:T(8,128)(2,1)} %wx.1, ...), custom_call_target="tpu_custom_call" | custom-call | tf_op jit(solution)/shard_map/pallas_call | solution.py:400
  110.0 0.0 slice-done
  110.0 1.5 %pad_maximum_fusion.2 = bf16[64,3,512]{2,0,1:T(8,128)(2,1)} fusion(bf16[64,1,512]{2,0,1:T(8,128)(2,1)} %bitcast.35, bf16[64,2,512]{2,0,1:T(8,128)(2,1)S(1)} %slice-done), kind=kLoop, calls=%fused_computation.9 | loop fusion | flops 98304 | bytes 393216 | tf_op jit(solution)/shard_map/concatenate | solution.py:417
  111.5 1.5 %copy.39 = bf16[64,512]{1,0:T(8,128)(2,1)} copy(bf16[64,512]{1,0:T(8,128)(2,1)} %get-tuple-element.14) | data formatting | bytes 131072
  113.0 1.6 %copy.40 = f32[64,512]{1,0:T(8,128)} copy(f32[64,512]{1,0:T(8,128)} %get-tuple-element.15) | data formatting | bytes 262144
  (7 shorter events, 0.1 us)
Async XLA Ops:
  0.6 7.9 %copy-start.1 = (bf16[512,768]{1,0:T(8,128)(2,1)S(1)}, bf16[512,768]{1,0:T(8,128)(2,1)}, u32[]{:S(2)}) copy-start(bf16[512,768]{1,0:T(8,128)(2,1)} %param.39) | copy-start | bytes 2359300
  10.8 2.3 %copy-start.4 = (bf16[2048]{0:T(1024)(128)(2,1)S(1)}, bf16[2048]{0:T(1024)(128)(2,1)}, u32[]{:S(2)}) copy-start(bf16[2048]{0:T(1024)(128)(2,1)} %param.22) | copy-start | bytes 12292
  10.8 2.3 %copy-start = (bf16[64,2048]{1,0:T(8,128)(2,1)S(1)}, bf16[64,2048]{1,0:T(8,128)(2,1)}, u32[]{:S(2)}) copy-start(bf16[64,2048]{1,0:T(8,128)(2,1)} %param.21) | copy-start | bytes 786436
  10.8 3.3 %copy-start.3 = (bf16[4,512]{1,0:T(4,128)(2,1)S(1)}, bf16[4,512]{1,0:T(4,128)(2,1)}, u32[]{:S(2)}) copy-start(bf16[4,512]{1,0:T(4,128)(2,1)} %param.25) | copy-start | bytes 12292
  10.8 3.3 %copy-start.2 = (bf16[64,3,512]{2,0,1:T(8,128)(2,1)S(1)}, bf16[64,3,512]{2,0,1:T(8,128)(2,1)}, u32[]{:S(2)}) copy-start(bf16[64,3,512]{2,0,1:T(8,128)(2,1)} %param.30) | copy-start | bytes 589828
  10.8 4.0 %copy-start.5 = (f32[512]{0:T(512)S(1)}, f32[512]{0:T(512)}, u32[]{:S(2)}) copy-start(f32[512]{0:T(512)} %param.28) | copy-start | bytes 6148
  16.0 94.0 %slice-start = ((bf16[64,3,512]{2,0,1:T(8,128)(2,1)}), bf16[64,2,512]{2,0,1:T(8,128)(2,1)S(1)}, s32[]{:S(2)}) async-start(bf16[64,3,512]{2,0,1:T(8,128)(2,1)} %param.30), calls=%async_computation | async-start | bytes 262144 | tf_op jit(solution)/shard_map/slice | solution.py:417

commit v2 on v1

v2 whole, which is shorter than its diff:
```python
import functools

import jax
import jax.numpy as jnp
from jax import lax
from jax.experimental import pallas as pl
from jax.experimental.pallas import tpu as pltpu
from jax.sharding import PartitionSpec as P

epsilon = 1e-06
decay_scale = 8.0
MESH = pl.DeviceIdType.MESH
F32 = jnp.float32
BF16 = jnp.bfloat16


def dot(a, b):
    return jnp.dot(a, b, preferred_element_type=F32)


def layer_kernel(
    E, T, slots,
    hidden, mix_gain, routes, weights, conv_old, taps, ig, dgate, decay_param, lru, ffn_gain, branch,
    wx_h, wy_h, dg_h, du_h, po_h, eg_h, eu_h, ed_h, dd_h,
    new_hidden, new_lru, x_out,
    ct, w_ref, bd, wx, wy, dg, du, po, eg, eu, ed, dd, nb, dwp, dwr, spread, pm, pacc, yrec, zout, zrec, ctr, acc,
    mbuf, mrec, qbuf, qrec, xall, hacc, aall, xe, hid, sel, ebuf, erec, dtmp, om, dacc, orm, oz, ozr,
    summed_ref,
    load_sem, nb_s, nb_r, ct_s, ct_r, pm_s, pm_r, pz_s, pz_r, dw_s, dw_r, mx_s, mx_r, q_s, q_r,
    xr_s, xm_s, x2_s, x1_s, x_r, a_s, a_r, er_s, er_r, om_s, om_r, oz_s, oz_r,
):
    e = lax.axis_index("ep")
    t = lax.axis_index("tp")
    M, D = hidden.shape
    C = D // T
    R = wx.shape[0]
    G = E // 2
    g0 = e // 2
    par = lax.rem(e, 2)
    mate = e + 1 - 2 * par
    own_cols = pl.ds(pl.multiple_of(t * C, 128), C)

    def ep_peer(k):
        return lax.rem(e + k, E)

    def ep_from(k):
        return lax.rem(e + E - k, E)

    def group(k):
        return lax.rem(g0 + k, G)

    def rail_from(k):
        return 2 * lax.rem(g0 + G - k, G) + par

    def mate_of(s):
        return s + 1 - 2 * lax.rem(s, 2)

    def tp_peer(k):
        return lax.rem(t + k, T)

    across = lax.rem(t + T // 2, T)
    beside = t + 1 - 2 * lax.rem(t, 2)
    diagonal = lax.rem(beside + T // 2, T)

    loads = [
        pltpu.make_async_copy(src, dst, load_sem.at[i])
        for i, (src, dst) in enumerate(
            ((po_h, po), (eg_h, eg), (eu_h, eu), (ed_h, ed), (dd_h, dd),
             (wx_h, wx), (wy_h, wy), (dg_h, dg), (du_h, du))
        )
    ]
    own_dw = pltpu.make_async_copy(dwp.at[t], dwr.at[t], load_sem.at[9])
    for i in (5, 6, 7, 8, 0):
        loads[i].start()

    def rcopy(src, dst, s, r, ep=None, tp=None):
        return pltpu.make_async_remote_copy(
            src_ref=src, dst_ref=dst, send_sem=s, recv_sem=r,
            device_id=(e if ep is None else ep, t if tp is None else tp),
            device_id_type=MESH,
        )

    barrier = pltpu.get_barrier_semaphore()

    @pl.loop(1, E)
    def _(k):
        pl.semaphore_signal(barrier, inc=1, device_id=(ep_peer(k), t), device_id_type=MESH)

    for k in range(1, T):
        pl.semaphore_signal(barrier, inc=1, device_id=(e, tp_peer(k)), device_id_type=MESH)
    hf = hidden[...].astype(F32)
    inv = lax.rsqrt(jnp.mean(hf * hf, axis=-1, keepdims=True) + epsilon)
    normed = (hf * inv * mix_gain[...].astype(F32)).astype(BF16)
    for p in range(E):
        nb[p] = normed[:, p * R:(p + 1) * R]
    for p in range(E):
        ct[p] = jnp.sum(jnp.where(routes[...] == p, weights[...], 0.0), axis=0, keepdims=True)
    pl.semaphore_wait(barrier, E - 1 + T - 1)

    @pl.loop(1, E)
    def _(k):
        p = ep_peer(k)
        rcopy(nb.at[p], spread.at[e], nb_s.at[p], nb_r.at[e], ep=p).start()
        rcopy(ct.at[p], ctr.at[e], ct_s.at[p], ct_r.at[e], ep=p).start()

    loads[7].wait()
    loads[8].wait()
    h = dg.shape[1] // T
    half = dwp.shape[2] // 2
    if half != h:
        dwp[...] = jnp.zeros_like(dwp)
    for j in range(T):
        dwp[j, :, :h] = dg[:, j * h:(j + 1) * h]
        dwp[j, :, half:half + h] = du[:, j * h:(j + 1) * h]
    own_dw.start()
    for k in range(1, T):
        j = tp_peer(k)
        rcopy(dwp.at[j], dwr.at[t], dw_s.at[j], dw_r.at[t], tp=j).start()
    for l in loads[1:5]:
        l.start()

    spread[e] = nb[e]
    loads[5].wait()
    loads[6].wait()

    def arrive(s):
        rcopy(nb.at[s], spread.at[s], nb_s.at[s], nb_r.at[s], ep=s).wait_recv()

    def share(g):
        blk = spread[2 * g + 1 - par]
        pm[g, :, :C] = dot(blk, wx[...]).astype(BF16)
        pm[g, :, C:] = dot(blk, wy[...]).astype(BF16)
        rcopy(pm.at[g], yrec.at[g], pm_s.at[g], pm_r.at[g], ep=mate).start()
        blk = spread[2 * g + par]
        pacc[g, :, :C] = dot(blk, wx[...])
        pacc[g, :, C:] = dot(blk, wy[...])

    def pass_on(g):
        rcopy(pm.at[g], yrec.at[g], pm_s.at[g], pm_r.at[g], ep=mate).wait_recv()
        zout[g] = (pacc[g] + yrec[g].astype(F32)).astype(BF16)
        rcopy(zout.at[g], zrec.at[g0], pz_s.at[g], pz_r.at[g0], ep=2 * g + par).start()

    @pl.loop(1, G)
    def _(k):
        g = group(k)
        arrive(2 * g + 1 - par)
        arrive(2 * g + par)
        share(g)

        @pl.when(k > 1)
        def _():
            pass_on(group(k - 1))

    arrive(mate)
    share(g0)
    pass_on(group(G - 1))

    @pl.loop(1, E)
    def _(k):
        s = ep_from(k)
        rcopy(ct.at[s], ctr.at[s], ct_s.at[s], ct_r.at[s], ep=s).wait_recv()

    ctr[e] = ct[e]
    N = E * M
    for s in range(E):
        w_ref[:, s * M:(s + 1) * M] = ctr[s]
    w_row = w_ref[...]
    bd[...] = jnp.zeros_like(bd)
    block = ig.shape[1]
    width = bd.shape[1]
    per = width // block
    for i in range(ig.shape[0]):
        lo = i % per * block
        bd[i // per, lo:lo + block, lo:lo + block] = ig[i]
        bd[i // per, lo:lo + block, width + lo:width + lo + block] = dgate[i]
    nblk = min(N, 512)
    tri = (
        lax.broadcasted_iota(jnp.int32, (nblk, nblk), 0)
        < lax.broadcasted_iota(jnp.int32, (nblk, nblk), 1)
    ).astype(F32).astype(BF16)
    base = jnp.zeros((1, 1), F32)
    w_slot = jnp.zeros((slots, 1), F32)
    for b in range(N // nblk):
        w_b = w_row[:, b * nblk:(b + 1) * nblk]
        m_b = (w_b > 0.0).astype(F32)
        rank = dot(jnp.broadcast_to(m_b, (16, nblk)).astype(BF16), tri)[0:1, :] + base
        base = base + jnp.sum(m_b, axis=1, keepdims=True)
        hit = (
            lax.broadcasted_iota(jnp.int32, (slots, nblk), 0).astype(F32) == rank
        ).astype(F32) * m_b
        sel[:, b * nblk:(b + 1) * nblk] = hit.astype(BF16)
        w_slot = w_slot + jnp.sum(hit * w_b, axis=1, keepdims=True)

    rcopy(pm.at[g0], yrec.at[g0], pm_s.at[g0], pm_r.at[g0], ep=mate).wait_recv()
    acc[...] = pacc[g0] + yrec[g0].astype(F32)

    @pl.loop(1, G)
    def _(k):
        g = group(k)
        rcopy(zout.at[g], zrec.at[g], pz_s.at[g], pz_r.at[g], ep=2 * g + par).wait_recv()
        acc[...] += zrec[g].astype(F32)

    x_b = acc[:, :C].astype(BF16)
    y_b = acc[:, C:].astype(BF16)
    x_out[...] = x_b
    conv_pre = conv_old[0].astype(F32) * taps[0:1, :].astype(F32)
    for i in range(1, taps.shape[0] - 1):
        conv_pre = conv_pre + conv_old[i].astype(F32) * taps[i:i + 1, :].astype(F32)
    conv = (conv_pre + x_b.astype(F32) * taps[taps.shape[0] - 1:, :].astype(F32)).astype(BF16)
    gi, gd = [], []
    for i in range(C // width):
        g = dot(conv[:, i * width:(i + 1) * width], bd[i])
        gi.append(g[:, :width])
        gd.append(g[:, width:])
    gate_in = jax.nn.sigmoid(jnp.concatenate(gi, axis=1))
    gate_dec = jax.nn.sigmoid(jnp.concatenate(gd, axis=1))
    dp = decay_param[...]
    log_decay = decay_scale * gate_dec * (jnp.minimum(dp, 0.0) - jnp.log1p(jnp.exp(-jnp.abs(dp))))
    decay = jnp.exp(log_decay)
    inject = jnp.sqrt(-jnp.tanh(log_decay) * (1.0 + decay * decay))
    state = decay * lru[...] + inject * gate_in * conv.astype(F32)
    new_lru[...] = state
    gated = (state * jax.nn.gelu(y_b.astype(F32), approximate=True)).astype(BF16)

    loads[0].wait()
    order = [tp_peer(k) for k in (2, 3, 1)] if T == 4 else [tp_peer(k) for k in range(1, T)]
    for j in order:
        cols = pl.ds(pl.multiple_of(j * C, 128), C)
        mbuf[j] = dot(gated, po[:, cols]).astype(BF16)
        rcopy(mbuf.at[j], mrec.at[t], mx_s.at[j], mx_r.at[t], tp=j).start()
    mixer = dot(gated, po[:, own_cols]).astype(BF16).astype(F32)
    for j in reversed(order):
        rcopy(mbuf.at[j], mrec.at[j], mx_s.at[j], mx_r.at[j], tp=j).wait_recv()
        mixer = mixer + mrec[j].astype(F32)
    summed = (hidden[:, own_cols].astype(F32) + mixer).astype(BF16)
    summed_ref[...] = summed
    sf = summed.astype(F32)
    ssq = jnp.sum(sf * sf, axis=1, keepdims=True)
    qbuf[...] = jnp.broadcast_to(ssq, qbuf.shape)
    for j in order:
        rcopy(qbuf, qrec.at[t], q_s.at[j], q_r.at[t], tp=j).start()
    total = qbuf[...]
    for j in reversed(order):
        rcopy(qbuf, qrec.at[j], q_s.at[j], q_r.at[j], tp=j).wait_recv()
        total = total + qrec[j]
    scale = lax.rsqrt(total[:, 0:1] * (1.0 / D) + epsilon)
    xall[t, e] = (sf * scale * ffn_gain[:, own_cols].astype(F32)).astype(BF16)

    def to_mate(s):
        rcopy(xall.at[t, s], xall.at[t, s], xm_s.at[s], x_r.at[t, s], ep=mate).start()

    @pl.loop(1, G)
    def _(k):
        g = group(k)
        rcopy(xall.at[t, e], xall.at[t, e], xr_s.at[g], x_r.at[t, e], ep=2 * g + par).start()

    to_mate(e)

    def spread_tp(s):
        rcopy(xall.at[t, s], xall.at[t, s], x2_s.at[s], x_r.at[t, s], tp=across).start()
        rcopy(xall.at[t, s], xall.at[t, s], x1_s.at[0, s], x_r.at[t, s], tp=beside).start()

    def forward(s):
        rcopy(xall.at[across, s], xall.at[across, s], x2_s.at[s], x_r.at[across, s], tp=across).wait_recv()
        rcopy(xall.at[across, s], xall.at[across, s], x1_s.at[1, s], x_r.at[across, s], tp=beside).start()

    def arrived(s, p):
        rcopy(xall.at[t, s], xall.at[t, s], xm_s.at[s], x_r.at[t, s], ep=p).wait_recv()

    spread_tp(e)

    @pl.loop(1, G)
    def _(k):
        s = rail_from(k)
        arrived(s, s)
        to_mate(s)
        spread_tp(s)
        last = mate_of(rail_from(k - 1))
        arrived(last, mate)
        spread_tp(last)
        forward(rail_from(k - 1))

        @pl.when(k > 1)
        def _():
            forward(mate_of(rail_from(k - 2)))

    last = mate_of(rail_from(G - 1))
    arrived(last, mate)
    spread_tp(last)
    forward(rail_from(G - 1))
    if G > 1:
        forward(mate_of(rail_from(G - 2)))
    forward(last)

    @pl.loop(0, E)
    def _(s):
        rcopy(xall.at[beside, s], xall.at[beside, s], x1_s.at[0, s], x_r.at[beside, s], tp=beside).wait_recv()
        rcopy(xall.at[diagonal, s], xall.at[diagonal, s], x1_s.at[1, s], x_r.at[diagonal, s], tp=beside).wait_recv()

    own_dw.wait()
    for j in order:
        rcopy(dwp.at[j], dwr.at[j], dw_s.at[j], dw_r.at[j], tp=j).wait_recv()
    rows = min(N, 512)

    @pl.loop(0, N // rows)
    def _(b):
        hacc[...] = jnp.zeros_like(hacc)
        eb = rows // M

        @pl.loop(0, T)
        def _(q):
            xq = xall[q, pl.ds(b * eb, eb)].reshape(rows, C)
            hacc[...] += dot(xq, dwr[q])

        h = hacc[...]
        half = h.shape[1] // 2
        act = jax.nn.silu(h) * pltpu.roll(h, half, axis=1)
        aall[t, pl.ds(pl.multiple_of(b * rows, 16), rows), :] = act[:, :half].astype(BF16)

    a_across = rcopy(aall.at[t], aall.at[t], a_s.at[0], a_r.at[t], tp=across)
    a_beside = rcopy(aall.at[t], aall.at[t], a_s.at[1], a_r.at[t], tp=beside)
    a_across.start()
    a_beside.start()

    @pl.loop(0, T)
    def _(q):
        cols = pl.ds(pl.multiple_of(q * C, 128), C)
        xe[:, cols] = dot(sel[...], xall[q].reshape(N, C)).astype(BF16)

    loads[1].wait()
    loads[2].wait()
    FH = eg.shape[1]
    nch = 256 if FH % 256 == 0 else FH

    @pl.loop(0, FH // nch)
    def _(n):
        cols = pl.ds(pl.multiple_of(n * nch, 128), nch)
        g = dot(xe[...], eg[:, cols])
        u = dot(xe[...], eu[:, cols])
        hid[:, cols] = (jax.nn.silu(g) * u).astype(BF16)

    a_in = rcopy(aall.at[across], aall.at[across], a_s.at[0], a_r.at[across], tp=across)
    a_in.wait_recv()
    a_fwd = rcopy(aall.at[across], aall.at[across], a_s.at[2], a_r.at[across], tp=beside)
    a_fwd.start()

    loads[3].wait()
    for j in order:
        cols = pl.ds(pl.multiple_of(j * C, 128), C)
        ebuf[j] = dot(hid[...], ed[:, cols]).astype(BF16)
        rcopy(ebuf.at[j], erec.at[t], er_s.at[j], er_r.at[t], tp=j).start()
    ebuf[t] = dot(hid[...], ed[:, own_cols]).astype(BF16)

    loads[4].wait()
    rcopy(aall.at[beside], aall.at[beside], a_s.at[1], a_r.at[beside], tp=beside).wait_recv()
    rcopy(aall.at[diagonal], aall.at[diagonal], a_s.at[2], a_r.at[diagonal], tp=beside).wait_recv()
    red = ebuf[t].astype(F32)
    for j in reversed(order):
        rcopy(ebuf.at[j], erec.at[j], er_s.at[j], er_r.at[j], tp=j).wait_recv()
        red = red + erec[j].astype(F32)
    red = (red.astype(BF16).astype(F32) * w_slot).astype(BF16)
    gate = jax.nn.sigmoid(branch[...])
    ebuf[t] = red
    pair = 2 * M

    def block(g):
        rws = pl.ds(pl.multiple_of(g * pair, 128 if pair % 128 == 0 else 16), pair)
        d = dot(aall[0, rws, :], dd[0])
        for q in range(1, T):
            d = d + dot(aall[q, rws, :], dd[q])
        d = d * gate + lax.dot_general(
            sel[:, rws], ebuf[t], (((0,), (0,)), ((), ())), preferred_element_type=F32
        )
        dtmp[...] = d.reshape(2, M, C)
        om[g] = dtmp[1 - par].astype(BF16)
        rcopy(om.at[g], orm.at[g], om_s.at[g], om_r.at[g], ep=mate).start()
        dacc[g] = dtmp[par]

    def block_on(g):
        rcopy(om.at[g], orm.at[g], om_s.at[g], om_r.at[g], ep=mate).wait_recv()
        oz[g] = (dacc[g] + orm[g].astype(F32)).astype(BF16)
        rcopy(oz.at[g], ozr.at[g0], oz_s.at[g], oz_r.at[g0], ep=2 * g + par).start()

    @pl.loop(1, G)
    def _(k):
        block(group(k))

        @pl.when(k > 1)
        def _():
            block_on(group(k - 1))

    block(g0)
    block_on(group(G - 1))
    rcopy(om.at[g0], orm.at[g0], om_s.at[g0], om_r.at[g0], ep=mate).wait_recv()
    acc[:, :C] = summed_ref[...].astype(F32) + dacc[g0] + orm[g0].astype(F32)

    @pl.loop(1, G)
    def _(k):
        g = group(k)
        rcopy(oz.at[g], ozr.at[g], oz_s.at[g], oz_r.at[g], ep=2 * g + par).wait_recv()
        acc[:, :C] += ozr[g].astype(F32)

    new_hidden[...] = acc[:, :C].astype(BF16)

    @pl.loop(1, E)
    def _(k):
        p = ep_peer(k)
        rcopy(nb.at[p], spread.at[e], nb_s.at[p], nb_r.at[e], ep=p).wait_send()
        rcopy(ct.at[p], ctr.at[e], ct_s.at[p], ct_r.at[e], ep=p).wait_send()

    @pl.loop(0, G)
    def _(g):
        rcopy(pm.at[g], yrec.at[g], pm_s.at[g], pm_r.at[g], ep=mate).wait_send()
        rcopy(om.at[g], orm.at[g], om_s.at[g], om_r.at[g], ep=mate).wait_send()
        s = 2 * g + par
        rcopy(xall.at[t, s], xall.at[t, s], xm_s.at[s], x_r.at[t, s], ep=mate).wait_send()

    @pl.loop(1, G)
    def _(k):
        g = group(k)
        p = 2 * g + par
        rcopy(zout.at[g], zrec.at[g0], pz_s.at[g], pz_r.at[g0], ep=p).wait_send()
        rcopy(oz.at[g], ozr.at[g0], oz_s.at[g], oz_r.at[g0], ep=p).wait_send()
        rcopy(xall.at[t, e], xall.at[t, e], xr_s.at[g], x_r.at[t, e], ep=p).wait_send()

    for j in order:
        rcopy(dwp.at[j], dwr.at[t], dw_s.at[j], dw_r.at[t], tp=j).wait_send()
        rcopy(mbuf.at[j], mrec.at[t], mx_s.at[j], mx_r.at[t], tp=j).wait_send()
        rcopy(qbuf, qrec.at[t], q_s.at[j], q_r.at[t], tp=j).wait_send()
        rcopy(ebuf.at[j], erec.at[t], er_s.at[j], er_r.at[t], tp=j).wait_send()

    @pl.loop(0, E)
    def _(s):
        rcopy(xall.at[t, s], xall.at[t, s], x2_s.at[s], x_r.at[t, s], tp=across).wait_send()
        rcopy(xall.at[t, s], xall.at[t, s], x1_s.at[0, s], x_r.at[t, s], tp=beside).wait_send()
        rcopy(xall.at[across, s], xall.at[across, s], x1_s.at[1, s], x_r.at[across, s], tp=beside).wait_send()

    a_across.wait_send()
    a_beside.wait_send()
    a_fwd.wait_send()


def on_device(
    hidden, mix_gain, proj_x, proj_y, conv_taps, input_gate, decay_gate, decay_param,
    proj_out, conv_state, lru_state, ffn_gain, routes, route_weights,
    expert_gate, expert_up, expert_down, dense_gate, dense_up, dense_down, branch_gate,
):
    E = lax.axis_size("ep")
    T = lax.axis_size("tp")
    M, D = hidden.shape
    C = D // T
    R = proj_x.shape[0]
    N = E * M
    heads, block = input_gate.shape[:2]
    group = max(1, 128 // block)

    experts = expert_gate.shape[0] * E
    capacity = M * routes.shape[1] // experts + 2
    slots = -(-E * capacity // 16) * 16
    G = E // 2
    h = dense_gate.shape[1] // T
    half = -(-2 * h // 128) * 64

    dd = jnp.pad(dense_down.reshape(T, h, C), ((0, 0), (0, half - h), (0, 0)))
    FH = expert_gate.shape[2]
    vm = pl.BlockSpec(memory_space=pltpu.VMEM)
    anyspace = pl.BlockSpec(memory_space=pl.ANY)
    DMA = pltpu.SemaphoreType.DMA
    V = pltpu.VMEM
    rows = min(N, 512)
    scratch = [
        V((E, 1, M), F32), V((1, N), F32), V((heads // group, group * block, 2 * group * block), BF16),
        V((R, C), BF16), V((R, C), BF16), V((C, T * h), BF16), V((C, T * h), BF16),
        V((C, D), BF16), V((D, FH), BF16), V((D, FH), BF16), V((FH, D), BF16), V((T, half, C), BF16),
        V((E, M, R), BF16), V((T, C, 2 * half), BF16), V((T, C, 2 * half), BF16),
        V((E, M, R), BF16), V((G, M, 2 * C), BF16), V((G, M, 2 * C), F32), V((G, M, 2 * C), BF16),
        V((G, M, 2 * C), BF16), V((G, M, 2 * C), BF16), V((E, 1, M), F32), V((M, 2 * C), F32),
        V((T, M, C), BF16), V((T, M, C), BF16), V((M, 128), F32), V((T, M, 128), F32),
        V((T, E, M, C), BF16), V((rows, 2 * half), F32), V((T, N, half), BF16),
        V((slots, D), BF16), V((slots, FH), BF16), V((slots, N), BF16),
        V((T, slots, C), BF16), V((T, slots, C), BF16), V((2, M, C), F32),
        V((G, M, C), BF16), V((G, M, C), F32), V((G, M, C), BF16), V((G, M, C), BF16), V((G, M, C), BF16),
        V((M, C), BF16),
        DMA((10,)),
        DMA((E,)), DMA((E,)), DMA((E,)), DMA((E,)), DMA((G,)), DMA((G,)), DMA((G,)), DMA((G,)),
        DMA((T,)), DMA((T,)), DMA((T,)), DMA((T,)), DMA((T,)), DMA((T,)),
        DMA((G,)), DMA((E,)), DMA((E,)), DMA((2, E)), DMA((T, E)), DMA((3,)), DMA((T,)), DMA((T,)), DMA((T,)),
        DMA((G,)), DMA((G,)), DMA((G,)), DMA((G,)),
    ]
    new_hidden, new_lru, x_new = pl.pallas_call(
        functools.partial(layer_kernel, E, T, slots),
        out_shape=(
            jax.ShapeDtypeStruct((M, C), BF16),
            jax.ShapeDtypeStruct((M, C), F32),
            jax.ShapeDtypeStruct((M, C), BF16),
        ),
        in_specs=[vm] * 12 + [anyspace] * 9,
        out_specs=(vm, vm, vm),
        scratch_shapes=scratch,
        compiler_params=pltpu.CompilerParams(
            collective_id=0, has_side_effects=True, vmem_limit_bytes=60 * 1024 * 1024
        ),
    )(
        hidden, mix_gain[None, :], routes.T, route_weights.T, conv_state.transpose(1, 0, 2), conv_taps,
        input_gate, decay_gate, decay_param[None, :], lru_state,
        ffn_gain[None, :], branch_gate[None, :],
        proj_x, proj_y, dense_gate, dense_up, proj_out, expert_gate[0], expert_up[0], expert_down[0], dd,
    )
    new_conv = jnp.concatenate([conv_state[:, 1:], x_new[:, None, :]], axis=1)
    return (new_hidden, new_lru, new_conv)


def solution(mesh):
    in_specs = (
        P("ep", None),
        P(),
        P("ep", "tp"),
        P("ep", "tp"),
        P(None, "tp"),
        P("tp", None, None),
        P("tp", None, None),
        P("tp"),
        P("tp", None),
        P("ep", None, "tp"),
        P("ep", "tp"),
        P(),
        P("ep", None),
        P("ep", None),
        P("ep", None, "tp"),
        P("ep", None, "tp"),
        P("ep", "tp", None),
        P("tp", "ep"),
        P("tp", "ep"),
        P("ep", "tp"),
        P("tp"),
    )
    out_specs = (P("ep", "tp"), P("ep", "tp"), P("ep", None, "tp"))
    return jax.shard_map(
        on_device, mesh=mesh, in_specs=in_specs, out_specs=out_specs, check_vma=False
    )
```

time: 116 us -> 96.5 us (0.83)
  other arithmetic: 8.29 us -> 1.54 us
  Pallas kernels: 93.9 us -> 87.4 us
  local copies, waits for them, and re-layouts: 11.5 us -> 6.53 us
    pallas_call x1, Pallas kernels: 93.9 us -> 87.4 us  [on_device(): pl.pallas_call(functools.partial(layer_kernel, E, T, slots), out_shape=(j...]
    mul x10 -> x0, local copies, waits for them, and re-layouts: 2.87 us -> none  [the longest x6 2.63 us: diag(): return (g * eye).reshape(heads // group, group * block, group * block)]
    broadcast_in_dim x0 -> x2, local copies, waits for them, and re-layouts: none -> 2.58 us  [the longest x1 1.29 us: on_device(): mix_gain[None, :]]
    concatenate x2 -> x0, other arithmetic: 2.48 us -> none  [the longest x1 1.74 us: on_device(): dwp = jnp.concatenate([cut(dense_gate), cut(dense_up)], axis=2)]
    reshape x3 -> x0, local copies, waits for them, and re-layouts: 1.74 us -> none  [the longest x2 1.02 us: cut(): w = w.reshape(C, T, h).transpose(1, 0, 2)]
    unnamed x16 -> x2, local copies, waits for them, and re-layouts: 4.77 us -> 3.04 us
    reduce_sum x3 -> x0, other arithmetic: 1.55 us -> none  [the longest x1 0.7 us: on_device(): jnp.sum(jnp.where(routes.T[None, :, :] == ids[:, None, None], route_weigh...]
    dynamic_slice x1 -> x0, local copies, waits for them, and re-layouts: 1.55 us -> none  [on_device(): hid_own = lax.dynamic_slice_in_dim(hidden, t * C, C, 1)]
where the time goes in v2:
time: 96.5 us; the launch traced here: 96.2 us
  Pallas kernels  87.4 us (91%)
  local copies, waits for them, and re-layouts  6.53 us (7%)
  other arithmetic  1.54 us (2%)
    pallas_call x1, Pallas kernels, on_device(): pl.pallas_call(functools.partial(layer_kernel, E, T, slots), out_shape=(j...  87.4 us
    unnamed x2, local copies, waits for them, and re-layouts  3.04 us

profile of v2, /device:TPU:0, one launch (start us, length us, event | category | flops | bytes accessed | tf_op | source)
XLA Modules:
  0.0 96.2 jit_solution(15235938616317857006)
XLA Ops:
  0.6 1.3 %broadcast_in_dim.15.mix_gain = bf16[1,2048]{1,0:T(2,128)(2,1)} reshape(bf16[2048]{0:T(1024)(128)(2,1)} %param.22) | data formatting | bytes 8192 | tf_op jit(solution)/shard_map/broadcast_in_dim | solution.py:504
  1.9 1.3 %broadcast_in_dim.17.ffn_gain = bf16[1,2048]{1,0:T(2,128)(2,1)} reshape(bf16[2048]{0:T(1024)(128)(2,1)} %param.32) | data formatting | bytes 8192 | tf_op jit(solution)/shard_map/broadcast_in_dim | solution.py:506
  3.2 0.9 slice.3
  4.1 87.4 %shard_map.220 = (bf16[64,512]{1,0:T(8,128)(2,1)}, f32[64,512]{1,0:T(8,128)}, bf16[64,512]{1,0:T(8,128)(2,1)}) custom-call(bf16[64,2048]{1,0:T(8,128)(2,1)} %hidden.1, bf16[1,2048]{1,0:T(2,128)(2,1)} %broadcast_in_dim.15.mix_gain, s32[2,64]{1,0:T(2,128)} %bitcast.18, f32[2,64]{1,0:T(2,128)} %bitcast.19, bf16[3,64,512]{2,1,0:T(8,128)(2,1)} %bitcast.14, ...), custom_call_target="tpu_custom_call" | custom-call | tf_op jit(solution)/shard_map/pallas_call | solution.py:490
  91.6 1.5 %pad_maximum_fusion = bf16[64,3,512]{2,0,1:T(8,128)(2,1)} fusion(bf16[64,1,512]{2,0,1:T(8,128)(2,1)} %bitcast.15, bf16[64,2,512]{2,0,1:T(8,128)(2,1)S(1)} %slice.3), kind=kLoop, calls=%fused_computation | loop fusion | flops 98304 | bytes 393216 | tf_op jit(solution)/shard_map/concatenate | solution.py:509
  93.1 1.5 %copy.26 = bf16[64,512]{1,0:T(8,128)(2,1)} copy(bf16[64,512]{1,0:T(8,128)(2,1)} %get-tuple-element.12) | data formatting | bytes 131072
  94.6 1.6 %copy.27 = f32[64,512]{1,0:T(8,128)} copy(f32[64,512]{1,0:T(8,128)} %get-tuple-element.13) | data formatting | bytes 262144
